TPU v7x, 32 devices: a whole 2x2x4 slice. The times are simulated.
32 devices in a mesh: sp: 8 (over z, x), tp: 4 (over y, core).
Axes of the slice: x: 2, y: 2, z: 4, core: 2. Of those that a mesh axis runs over, the one named last changes fastest.
Arguments:
- residual: bfloat16 [2048, 2048], P(('sp', 'tp')), may hold values from -6 to 6
- query_wide: bfloat16 [2048, 512], P('sp', 'tp'), may hold values from -8 to 8
- key_wide: bfloat16 [2048, 512], P('sp', 'tp'), may hold values from -8 to 8
- value_wide: bfloat16 [2048, 512], P('sp', 'tp'), may hold values from -6 to 6
- query_narrow: bfloat16 [2048, 512], P('sp', 'tp'), may hold values from -8 to 8
- key_narrow: bfloat16 [2048, 512], P('sp', 'tp'), may hold values from -8 to 8
- value_narrow: bfloat16 [2048, 512], P('sp', 'tp'), may hold values from -6 to 6
- gate_wide: float32 [2048, 4], P('sp', 'tp'), may hold values from -2 to 20
- gate_narrow: float32 [2048, 8], P('sp', 'tp'), may hold values from -2 to 20
- out_wide: bfloat16 [512, 2048], replicated, may hold values from -0.1875 to 0.1875
- out_narrow: bfloat16 [512, 2048], replicated, may hold values from -0.1875 to 0.1875
- norm_gain: float32 [2048], replicated, may hold values from 0.1 to 1.9
- routing: int32 [2048, 2], P(('sp', 'tp')), may hold values from 0 to 7, as said below
- route_weight: float32 [2048, 2], P(('sp', 'tp')), may hold values from 0.3 to 1.5
- gate_weight: bfloat16 [8, 2048, 1024], P('sp', None, 'tp'), may hold values from -0.125 to 0.125
- up_weight: bfloat16 [8, 2048, 1024], P('sp', None, 'tp'), may hold values from -0.125 to 0.125
- down_weight: bfloat16 [8, 1024, 2048], P('sp', 'tp'), may hold values from -0.1875 to 0.1875
Outputs:
- result: bfloat16 [2048, 2048], P(('sp', 'tp'))
Inputs may be any that keep to these rules, and one draw needn't show every extreme that they name: `routing`: each row names 2 different experts of one group (experts g * 2 to g * 2 + 1). In each aligned block of 64 rows (the rows of one device) no expert is named by more than 32 rows; one group, the same for all blocks, has each of its experts named by exactly 32 rows of every block.
All inputs are finite; a program needn't handle non-finite values.
Results may differ from a plain program's by a relative error of at most 0.017.
Values may be sent and summed in bfloat16 or wider, within the bound.
A program may use at most 128 MiB of HBM per device.

v0:
```python
import math
import jax
import jax.numpy as jnp
from jax import lax
from jax.sharding import PartitionSpec as P

HW = 128
HN = 64
GROUPS = 4
epsilon = 1e-06


def globalize(pieces, shard_rows):
    shards = pieces.shape[0] // shard_rows
    grid = pieces.reshape(shards, shard_rows, pieces.shape[1])
    endings = grid[:, -1, :]
    offsets = jnp.cumsum(endings, axis=0) - endings
    return (grid + offsets[:, None, :]).reshape(pieces.shape)


def head_block(
    state, queries, query_decay, keys, values, key_decay, first_key, first_query, head_width
):
    highest_old, weight_sum, weighted = state
    query_rows = queries.shape[0]
    head_count = query_decay.shape[1]
    key_rows = keys.shape[0]
    grid_query = queries.reshape(query_rows, head_count, head_width)
    grid_key = keys.reshape(key_rows, head_count, head_width)
    grid_value = values.reshape(key_rows, head_count, head_width)
    scores = jnp.einsum("thd,phd->htp", grid_query, grid_key, preferred_element_type=jnp.float32)
    scores = scores * head_width ** (-0.5) + query_decay.T[:, :, None] - key_decay.T[:, None, :]
    query_place = first_query + jnp.arange(query_rows, dtype=jnp.int32)
    key_place = first_key + jnp.arange(key_rows, dtype=jnp.int32)
    scores = jnp.where(key_place[None, None, :] <= query_place[None, :, None], scores, -jnp.inf)
    highest = jnp.maximum(highest_old, jnp.max(scores, axis=2))
    weights = jnp.exp(scores - highest[:, :, None])
    shrink = jnp.exp(highest_old - highest)
    weight_sum = weight_sum * shrink + jnp.sum(weights, axis=2)
    product = jnp.einsum(
        "htp,phd->htd", weights.astype(jnp.bfloat16), grid_value, preferred_element_type=jnp.float32
    )
    weighted = weighted * shrink[:, :, None] + product
    return (highest, weight_sum, weighted)


def fresh_state(head_count, shard_rows, head_width):
    return (
        jnp.full((head_count, shard_rows), -1e30, jnp.float32),
        jnp.zeros((head_count, shard_rows), jnp.float32),
        jnp.zeros((head_count, shard_rows, head_width), jnp.float32),
    )


def finish(state, shard_rows):
    highest, weight_sum, weighted = state
    mixed_heads = weighted / weight_sum[:, :, None]
    joined = jnp.transpose(mixed_heads, (1, 0, 2))
    return joined.reshape(shard_rows, weighted.shape[0] * weighted.shape[2]).astype(jnp.bfloat16)


def body(
    residual,
    query_wide,
    key_wide,
    value_wide,
    query_narrow,
    key_narrow,
    value_narrow,
    gate_wide,
    gate_narrow,
    out_wide,
    out_narrow,
    norm_gain,
    routing,
    route_weight,
    gate_weight,
    up_weight,
    down_weight,
):
    shard_rows = query_wide.shape[0]
    half_rows = shard_rows // 2
    sp_place = lax.axis_index("sp")
    first_query = sp_place * shard_rows
    running_wide = jnp.cumsum(jax.nn.log_sigmoid(gate_wide), axis=0)
    running_narrow = jnp.cumsum(jax.nn.log_sigmoid(gate_narrow), axis=0)
    pieces_wide, pieces_narrow = (
        lax.all_gather(running_wide, "sp", axis=0, tiled=True),
        lax.all_gather(running_narrow, "sp", axis=0, tiled=True),
    )
    every_wide = globalize(pieces_wide, shard_rows)
    every_narrow = globalize(pieces_narrow, shard_rows)
    late_first = first_query + half_rows
    halves = []
    for place, part_wide, part_narrow in (
        (first_query, query_wide[:half_rows], query_narrow[:half_rows]),
        (late_first, query_wide[half_rows:], query_narrow[half_rows:]),
    ):
        halves.append(
            (
                place,
                part_wide,
                part_narrow,
                lax.dynamic_slice_in_dim(every_wide, place, half_rows, 0),
                lax.dynamic_slice_in_dim(every_narrow, place, half_rows, 0),
            )
        )

    def half_state():
        return (
            fresh_state(gate_wide.shape[1], half_rows, HW),
            fresh_state(gate_narrow.shape[1], half_rows, HN),
        )

    state = (half_state(), half_state())
    keys_wide = lax.all_gather(key_wide, "sp", axis=0, tiled=True)
    values_wide = lax.all_gather(value_wide, "sp", axis=0, tiled=True)
    keys_narrow = lax.all_gather(key_narrow, "sp", axis=0, tiled=True)
    values_narrow = lax.all_gather(value_narrow, "sp", axis=0, tiled=True)
    span_rows = keys_wide.shape[0]
    block_size = math.gcd(span_rows, 2048)

    def visit(carried, position):
        inside = position * block_size

        def take_block(source):
            return lax.dynamic_slice_in_dim(source, inside, block_size, 0)

        def take_decay(source):
            return lax.dynamic_slice_in_dim(source, inside, block_size, 0)

        block_kw = take_block(keys_wide)
        block_vw = take_block(values_wide)
        block_kn = take_block(keys_narrow)
        block_vn = take_block(values_narrow)
        block_dw = take_decay(every_wide)
        block_dn = take_decay(every_narrow)

        def one_half(current, half):
            place, part_wide, part_narrow, query_decay_wide, query_decay_narrow = half

            def work(inner):
                first = head_block(
                    inner[0],
                    part_wide,
                    query_decay_wide,
                    block_kw,
                    block_vw,
                    block_dw,
                    inside,
                    place,
                    HW,
                )
                second = head_block(
                    inner[1],
                    part_narrow,
                    query_decay_narrow,
                    block_kn,
                    block_vn,
                    block_dn,
                    inside,
                    place,
                    HN,
                )
                return (first, second)

            def skip(inner):
                return inner

            return lax.cond(inside <= place + half_rows - 1, work, skip, current)

        updated = (one_half(carried[0], halves[0]), one_half(carried[1], halves[1]))
        return (updated, None)

    state, _ = lax.scan(visit, state, jnp.arange(span_rows // block_size, dtype=jnp.int32))
    att_wide = jnp.concatenate(
        [finish(state[0][0], half_rows), finish(state[1][0], half_rows)], axis=0
    )
    att_narrow = jnp.concatenate(
        [finish(state[0][1], half_rows), finish(state[1][1], half_rows)], axis=0
    )
    own_rows = residual.shape[0]
    tp_place = lax.axis_index("tp")
    rows_wide = lax.dynamic_slice_in_dim(
        out_wide, tp_place * att_wide.shape[1], att_wide.shape[1], 0
    )
    rows_narrow = lax.dynamic_slice_in_dim(
        out_narrow, tp_place * att_narrow.shape[1], att_narrow.shape[1], 0
    )
    first = jnp.dot(att_wide, rows_wide, preferred_element_type=jnp.float32)
    second = jnp.dot(att_narrow, rows_narrow, preferred_element_type=jnp.float32)
    mixed = lax.psum_scatter(
        (first + second).astype(jnp.bfloat16), "tp", scatter_dimension=0, tiled=True
    ).astype(jnp.float32)
    middle = (residual.astype(jnp.float32) + mixed).astype(jnp.bfloat16)
    middle_wide = middle.astype(jnp.float32)
    spread = jnp.mean(middle_wide * middle_wide, axis=1, keepdims=True)
    normed = (middle_wide * lax.rsqrt(spread + epsilon) * norm_gain).astype(jnp.bfloat16)
    features = normed.shape[1]
    chosen_count = routing.shape[1]
    expert_count = gate_weight.shape[0] * lax.axis_size("sp")
    capacity = own_rows * GROUPS // expert_count
    flat_routes = routing.reshape(-1)
    matches = (flat_routes[:, None] == jnp.arange(expert_count, dtype=jnp.int32)[None, :]).astype(
        jnp.int32
    )
    ranking = jnp.sum((jnp.cumsum(matches, axis=0) - matches) * matches, axis=1)
    placing = flat_routes * capacity + ranking
    picker = (
        placing[None, :] == jnp.arange(expert_count * capacity, dtype=jnp.int32)[:, None]
    ).astype(jnp.bfloat16)
    picker = jnp.sum(picker.reshape(expert_count * capacity, own_rows, chosen_count), axis=2)
    outgoing = jnp.dot(picker, normed, preferred_element_type=jnp.float32).astype(jnp.bfloat16)
    outgoing = outgoing.reshape(expert_count, capacity, features)
    arrived = lax.all_to_all(outgoing, "sp", split_axis=0, concat_axis=0, tiled=True)
    pooled = lax.all_gather(arrived.reshape(-1, features), "tp", axis=0, tiled=True)
    gate_value = jnp.dot(pooled, gate_weight[0], preferred_element_type=jnp.float32)
    up_value = jnp.dot(pooled, up_weight[0], preferred_element_type=jnp.float32)
    hidden = (jax.nn.silu(gate_value) * up_value).astype(jnp.bfloat16)
    answers = lax.psum_scatter(
        jnp.dot(hidden, down_weight[0], preferred_element_type=jnp.float32).astype(jnp.bfloat16),
        "tp",
        scatter_dimension=0,
        tiled=True,
    )
    returned = lax.all_to_all(
        answers.reshape(expert_count, capacity, features),
        "sp",
        split_axis=0,
        concat_axis=0,
        tiled=True,
    )
    picked = jnp.take(returned.reshape(expert_count * capacity, features), placing, axis=0)
    picked = picked.reshape(own_rows, chosen_count, features).astype(jnp.float32)
    combined = jnp.sum(route_weight[:, :, None] * picked, axis=1)
    return (middle_wide + combined).astype(jnp.bfloat16)


def solution(mesh):
    placed = (
        P(("sp", "tp"), None),
        P("sp", "tp"),
        P("sp", "tp"),
        P("sp", "tp"),
        P("sp", "tp"),
        P("sp", "tp"),
        P("sp", "tp"),
        P("sp", "tp"),
        P("sp", "tp"),
        P(),
        P(),
        P(),
        P(("sp", "tp"), None),
        P(("sp", "tp"), None),
        P("sp", None, "tp"),
        P("sp", None, "tp"),
        P("sp", "tp", None),
    )
    return jax.shard_map(
        body, mesh=mesh, in_specs=placed, out_specs=P(("sp", "tp"), None), check_vma=False
    )
```

profile of v0, /device:TPU:0, one launch (start us, length us, event | category | flops | bytes accessed | tf_op | source)
XLA Modules:
  0.0 408.9 jit_solution(1248506105477989104)
XLA Ops:
  8.5 27.9 %all_gather.25 = f32[2048,2]{0,1:T(2,128)S(1)} all-gather(f32[256,2]{0,1:T(2,128)S(1)} %bitcast.168), channel_id=1, replica_groups=mesh['sp'=8,'tp'=4] {'sp'}, dimensions={0}, use_global_device_ids=true | all-gather | bytes 18432 | tf_op jit(solution)/shard_map/all_gather | solution.py:89
  38.3 19.0 %all_gather.22 = f32[2048,1]{0,1:T(1,128)S(1)} all-gather(f32[256,1]{0,1:T(1,128)S(1)} %reduce_window_sum.69), channel_id=1, replica_groups=mesh['sp'=8,'tp'=4] {'sp'}, dimensions={0}, use_global_device_ids=true | all-gather | bytes 9216 | tf_op jit(solution)/shard_map/all_gather | solution.py:88
  59.3 33.5 %all_gather.24 = bf16[2048,128]{0,1:T(8,128)(2,1)} all-gather(bf16[256,128]{0,1:T(8,128)(2,1)S(1)} %copy.47), channel_id=1, replica_groups=mesh['sp'=8,'tp'=4] {'sp'}, dimensions={0}, use_global_device_ids=true | all-gather | bytes 589824 | tf_op jit(solution)/shard_map/all_gather | solution.py:118
  93.7 31.4 %all_gather.26 = bf16[2048,128]{0,1:T(8,128)(2,1)S(1)} all-gather(bf16[256,128]{0,1:T(8,128)(2,1)S(1)} %copy.49), channel_id=1, replica_groups=mesh['sp'=8,'tp'=4] {'sp'}, dimensions={0}, use_global_device_ids=true | all-gather | bytes 589824 | tf_op jit(solution)/shard_map/all_gather | solution.py:119
  125.1 33.7 %all_gather.21 = bf16[2048,128]{1,0:T(8,128)(2,1)} all-gather(bf16[256,128]{1,0:T(8,128)(2,1)} %param.23), channel_id=1, replica_groups=mesh['sp'=8,'tp'=4] {'sp'}, dimensions={0}, use_global_device_ids=true | all-gather | bytes 589824 | tf_op jit(solution)/shard_map/all_gather | solution.py:116
  158.9 31.2 %all_gather.23 = bf16[2048,128]{1,0:T(8,128)(2,1)S(1)} all-gather(bf16[256,128]{1,0:T(8,128)(2,1)S(1)} %copy-done.5), channel_id=1, replica_groups=mesh['sp'=8,'tp'=4] {'sp'}, dimensions={0}, use_global_device_ids=true | all-gather | bytes 589824 | tf_op jit(solution)/shard_map/all_gather | solution.py:117
  192.3 10.5 %conditional.3 = (f32[1,128]{1,0:T(1,128)S(1)}, f32[1,128,128]{2,1,0:T(8,128)S(1)}, f32[2,128]{1,0:T(2,128)}, f32[2,128,64]{1,2,0:T(8,128)}) conditional(s32[]{:T(128)} %convert_element_type.106, (f32[1,128]{1,0:T(1,128)}, f32[1,128,128]{2,1,0:T(8,128)S(1)}, f32[2,128]{1,0:T(2,128)}, f32[2,128,64]{1,2,0:T(8,128)S(1)}) %tuple.35, (s32[]{:T(128)}, ...), branch_computations={%region_12.13_spmd, %region_13.18_spmd.clone} | conditional | flops 276104320 | bytes 15037726 | solution.py:170
  193.7 1.6 copy.51
  196.1 1.9 fusion.86
  203.3 8.7 %conditional.2 = ((f32[1,128]{1,0:T(1,128)}, f32[1,128,128]{2,1,0:T(8,128)S(1)}, f32[2,128]{1,0:T(2,128)}, f32[2,128,64]{1,2,0:T(8,128)S(1)})) conditional(s32[]{:T(128)} %convert_element_type.103, (f32[1,128]{1,0:T(1,128)}, f32[1,128,128]{2,1,0:T(8,128)S(1)}, f32[2,128]{1,0:T(2,128)}, f32[2,128,64]{1,2,0:T(8,128)S(1)}) %tuple.35, (s32[]{:T(128)}, ...), branch_computations={%region_6.7_spmd, %region_7.12_spmd.clone} | conditional | flops 276104320 | bytes 15033570 | solution.py:170
  205.2 1.9 fusion.84
  214.7 2.5 fusion.38
  218.3 21.2 %reduce-scatter.3.cloned.1.call-done = bf16[64,2048]{1,0:T(8,128)(2,1)} async-done(((bf16[256,2048]{1,0:T(8,128)(2,1)}), bf16[64,2048]{1,0:T(8,128)(2,1)}) %reduce-scatter.3.cloned.1.call-update) | async-done | bytes 262160 | tf_op jit(solution)/shard_map/reduce_scatter | solution.py:192
  240.7 1.4 convolution_convert_fusion.1
  242.2 31.1 %all_to_all.10 = bf16[8,32,2048]{2,1,0:T(8,128)(2,1)} all-to-all(bf16[8,32,2048]{2,1,0:T(8,128)(2,1)S(1)} %bitcast.150), channel_id=1, replica_groups=mesh['sp'=8,'tp'=4] {'sp'}, dimensions={0} | all-to-all | bytes 2097152 | tf_op jit(solution)/shard_map/all_to_all | solution.py:215
  273.6 32.5 %all-gather.2.cloned.1.call-done = bf16[1024,2048]{1,0:T(8,128)(2,1)} async-done(((bf16[256,2048]{1,0:T(8,128)(2,1)}), bf16[1024,2048]{1,0:T(8,128)(2,1)}) %all-gather.2.cloned.1.call-update) | async-done | bytes 4194320 | tf_op jit(solution)/shard_map/all_gather | solution.py:216
  306.0 4.5 %fusion.43 = f32[1024,256]{1,0:T(8,128)} fusion(bf16[1024,2048]{1,0:T(8,128)(2,1)} %all-gather.2.cloned.1.call-done, bf16[1,2048,256]{2,1,0:T(8,128)(2,1)S(1)} %copy-done.18), kind=kOutput, calls=%fused_computation.73 | convolution fusion | flops 1073741824 | bytes 6291456 | tf_op jit(solution)/shard_map/dot_general | solution.py:217
  310.5 9.4 %convolution_convert_fusion = bf16[1024,2048]{1,0:T(8,128)(2,1)} fusion(bf16[1024,2048]{1,0:T(8,128)(2,1)} %all-gather.2.cloned.1.call-done, bf16[1,256,2048]{2,1,0:T(8,128)(2,1)} %param.37, bf16[1,2048,256]{2,1,0:T(8,128)(2,1)} %param.36, f32[1024,256]{1,0:T(8,128)} %fusion.43), kind=kOutput, calls=%fused_computation.65 | convolution fusion | flops 2151153664 | bytes 11534336 | tf_op jit(solution)/shard_map/dot_general | solution.py:221
  320.0 44.7 %reduce-scatter.5.cloned.1.call-done = bf16[256,2048]{1,0:T(8,128)(2,1)} async-done(((bf16[1024,2048]{1,0:T(8,128)(2,1)}), bf16[256,2048]{1,0:T(8,128)(2,1)}) %reduce-scatter.5.cloned.1.call-update) | async-done | bytes 1048592 | tf_op jit(solution)/shard_map/reduce_scatter | solution.py:220
  364.7 5.5 %all-to-all-start.1 = ((bf16[8,32,2048]{2,1,0:T(8,128)(2,1)}), bf16[8,32,2048]{2,1,0:T(8,128)(2,1)S(1)}, u32[]{:S(2)}, u32[]{:S(2)}) async-start(bf16[8,32,2048]{2,1,0:T(8,128)(2,1)} %bitcast.151), calls=%async_computation.3 | async-start | bytes 2097152 | tf_op jit(solution)/shard_map/all_to_all | solution.py:226
  370.7 25.2 %all-to-all-done.1 = bf16[8,32,2048]{2,1,0:T(8,128)(2,1)S(1)} async-done(((bf16[8,32,2048]{2,1,0:T(8,128)(2,1)}), bf16[8,32,2048]{2,1,0:T(8,128)(2,1)S(1)}, u32[]{:S(2)}, u32[]{:S(2)}) %all-to-all-start.1) | async-done | bytes 1048608 | tf_op jit(solution)/shard_map/all_to_all | solution.py:226
  395.9 1.7 gather_fusion
  397.6 1.4 gather.7
  399.0 2.5 multiply_reduce_fusion
  (138 shorter events, 29.5 us)
Async XLA Ops:
  6.5 207.7 %copy-start = (bf16[512,2048]{1,0:T(8,128)(2,1)S(1)}, bf16[512,2048]{1,0:T(8,128)(2,1)}, u32[]{:S(2)}) copy-start(bf16[512,2048]{1,0:T(8,128)(2,1)} %param.30) | copy-start | bytes 6291460
  6.5 152.3 %copy-start.5 = (bf16[256,128]{1,0:T(8,128)(2,1)S(1)}, bf16[256,128]{1,0:T(8,128)(2,1)}, u32[]{:S(2)}) copy-start(bf16[256,128]{1,0:T(8,128)(2,1)} %param.24) | copy-start | bytes 196612
  6.5 233.0 %reduce-scatter.3.cloned.1.call-start = ((), (), s32[]{:S(2)}) async-start(), calls=%async_computation.4 | async-start | bytes 1310720 | tf_op jit(solution)/shard_map/reduce_scatter | solution.py:192
  192.9 0.6 copy-start.15
  195.3 2.6 copy-start.6
  198.0 2.9 copy-start.10
  198.0 3.0 copy-start.3
  198.0 3.0 copy-start.16
  198.0 3.0 copy-start.19
  199.7 1.8 copy-start.12
  203.4 3.8 copy-start.7
  207.2 2.3 copy-start.11
  207.2 2.4 copy-start.4
  207.2 2.4 copy-start.20
  208.9 1.2 copy-start.13
  214.7 2.7 copy-start.8
  214.7 24.9 %copy-start.1 = (bf16[64,2048]{1,0:T(8,128)(2,1)S(1)}, bf16[64,2048]{1,0:T(8,128)(2,1)}, u32[]{:S(2)}) copy-start(bf16[64,2048]{1,0:T(8,128)(2,1)} %param.21) | copy-start | bytes 786436
  214.7 26.0 %copy-start.9 = (f32[2048]{0:T(1024)S(1)}, f32[2048]{0:T(1024)}, u32[]{:S(2)}) copy-start(f32[2048]{0:T(1024)} %param.32) | copy-start | bytes 24580
  217.3 88.8 %all-gather.2.cloned.1.call-start = ((), (), s32[]{:S(2)}) async-start(), calls=%async_computation.5 | async-start | bytes 5242880 | tf_op jit(solution)/shard_map/all_gather | solution.py:216
  242.1 63.9 %copy-start.18 = (bf16[1,2048,256]{2,1,0:T(8,128)(2,1)S(1)}, bf16[1,2048,256]{2,1,0:T(8,128)(2,1)}, u32[]{:S(2)}) copy-start(bf16[1,2048,256]{2,1,0:T(8,128)(2,1)} %param.35) | copy-start | bytes 3145732
  273.3 91.4 %reduce-scatter.5.cloned.1.call-start = ((), (), s32[]{:S(2)}) async-start(), calls=%async_computation.6 | async-start | bytes 5242880 | tf_op jit(solution)/shard_map/reduce_scatter | solution.py:220
  320.0 50.6 %copy-start.14 = (f32[64,2]{0,1:T(2,128)S(1)}, f32[64,2]{0,1:T(2,128)}, u32[]{:S(2)}) copy-start(f32[64,2]{0,1:T(2,128)} %param.34) | copy-start | bytes 1540
  364.7 31.2 %all-to-all-start.1 = ((bf16[8,32,2048]{2,1,0:T(8,128)(2,1)}), bf16[8,32,2048]{2,1,0:T(8,128)(2,1)S(1)}, u32[]{:S(2)}, u32[]{:S(2)}) async-start(bf16[8,32,2048]{2,1,0:T(8,128)(2,1)} %bitcast.151), calls=%async_computation.3 | async-start | bytes 2097152 | tf_op jit(solution)/shard_map/all_to_all | solution.py:226
  397.6 4.0 copy-start.2
  (1 other events, 0.5 us)
Sparse Core Ops, SparseCore 0:
  217.4 22.1 reduce-scatter.2
  273.5 32.5 all-gather.1
  320.1 44.5 reduce-scatter.4
where the time goes:
time: 410 us; the launch traced here: 409 us
  blocking collectives  208 us (51%)
  waiting for transfers between devices  124 us (30%)
  matrix products  25.6 us (6%)
  other arithmetic  18.2 us (4%)
  local copies, waits for them, and re-layouts  14.4 us (4%)
  between operations  13.4 us (3%)
  starting transfers between devices  5.77 us (1%)
    reduce_scatter x1, waiting for transfers between devices, body(): lax.psum_scatter(jnp.dot(hidden, down_weight[0], preferred_element_type=j...  44.7 us
    all_gather x1, blocking collectives, body(): keys_wide = lax.all_gather(key_wide, 'sp', axis=0, tiled=True)  33.7 us
    all_gather x1, blocking collectives, body(): keys_narrow = lax.all_gather(key_narrow, 'sp', axis=0, tiled=True)  33.5 us
    all_gather x1, waiting for transfers between devices, body(): lax.all_gather(arrived.reshape(-1, features), 'tp', axis=0, tiled=True)  32.5 us
    all_gather x1, blocking collectives, body(): values_narrow = lax.all_gather(value_narrow, 'sp', axis=0, tiled=True)  31.4 us
    all_gather x1, blocking collectives, body(): values_wide = lax.all_gather(value_wide, 'sp', axis=0, tiled=True)  31.2 us
    all_to_all x1, blocking collectives, body(): lax.all_to_all(outgoing, 'sp', split_axis=0, concat_axis=0, tiled=True)  31.1 us
    all_gather x1, blocking collectives, body(): lax.all_gather(running_narrow, 'sp', axis=0, tiled=True)  27.9 us
  transfers between devices with their start and end apart: 4, of which 4 were waited for; matrix products, arithmetic and copies ran while one was open for 0% of the time, Pallas kernels for 0%

commit v1 on v0

--- a/solution.py
+++ b/solution.py
@@ -8,6 +8,16 @@
 HN = 64
 GROUPS = 4
 epsilon = 1e-06
+
+
+def gather_by_hops(x, axis, d):
+    size = lax.axis_size(axis)
+    held, blocks = (x, [x])
+    for _ in range(size - 1):
+        held = lax.ppermute(held, axis, [(i, (i + 1) % size) for i in range(size)])
+        blocks.insert(0, held)
+    merged = jnp.concatenate(blocks, axis=d)
+    return jnp.roll(merged, (lax.axis_index(axis) + 1) * x.shape[d], axis=d)
 
 
 def globalize(pieces, shard_rows):
@@ -113,7 +123,7 @@
         )
 
     state = (half_state(), half_state())
-    keys_wide = lax.all_gather(key_wide, "sp", axis=0, tiled=True)
+    keys_wide = gather_by_hops(key_wide, "sp", 0)
     values_wide = lax.all_gather(value_wide, "sp", axis=0, tiled=True)
     keys_narrow = lax.all_gather(key_narrow, "sp", axis=0, tiled=True)
     values_narrow = lax.all_gather(value_narrow, "sp", axis=0, tiled=True)

time: 410 us -> 428 us (1.044)
  blocking collectives: 208 us -> 175 us
  waiting for transfers between devices: 124 us -> 153 us
  local copies, waits for them, and re-layouts: 14.4 us -> 28.1 us
    all_gather x1 -> x0, blocking collectives: 33.7 us -> none  [body(): keys_wide = lax.all_gather(key_wide, 'sp', axis=0, tiled=True)]
    ppermute x0 -> x7, waiting for transfers between devices: none -> 27.5 us  [gather_by_hops(): held = lax.ppermute(held, axis, [(i, (i + 1) % size) for i in range(size)])]
    unnamed x31 -> x58, local copies, waits for them, and re-layouts: 2.97 us -> 13.8 us
  transfers between devices with their start and end apart: 4 -> 11, of which waited for: 4 -> 9; matrix products, arithmetic and copies ran while one was open for 0% -> 4% of each run, Pallas kernels for 0% -> 0%
where the time goes in v1:
time: 428 us; the launch traced here: 427 us
  blocking collectives  175 us (41%)
  waiting for transfers between devices  153 us (36%)
  local copies, waits for them, and re-layouts  28.1 us (7%)
  matrix products  25.6 us (6%)
  other arithmetic  22.1 us (5%)
  between operations  13.4 us (3%)
  starting transfers between devices  8.87 us (2%)
    reduce_scatter x1, waiting for transfers between devices, body(): lax.psum_scatter(jnp.dot(hidden, down_weight[0], preferred_element_type=j...  44.7 us
    all_gather x1, blocking collectives, body(): keys_narrow = lax.all_gather(key_narrow, 'sp', axis=0, tiled=True)  33.6 us
    all_gather x1, waiting for transfers between devices, body(): lax.all_gather(arrived.reshape(-1, features), 'tp', axis=0, tiled=True)  32.5 us
    all_gather x1, blocking collectives, body(): values_narrow = lax.all_gather(value_narrow, 'sp', axis=0, tiled=True)  31.6 us
    all_gather x1, blocking collectives, body(): values_wide = lax.all_gather(value_wide, 'sp', axis=0, tiled=True)  31.4 us
    all_to_all x1, blocking collectives, body(): lax.all_to_all(outgoing, 'sp', split_axis=0, concat_axis=0, tiled=True)  31.1 us
    ppermute x7, waiting for transfers between devices, gather_by_hops(): held = lax.ppermute(held, axis, [(i, (i + 1) % size) for i in range(size)])  27.5 us
    all_gather x1, blocking collectives, body(): lax.all_gather(running_narrow, 'sp', axis=0, tiled=True)  26.4 us
  transfers between devices with their start and end apart: 11, of which 9 were waited for; matrix products, arithmetic and copies ran while one was open for 4% of the time, Pallas kernels for 0%

profile of v1, /device:TPU:0, one launch (start us, length us, event | category | flops | bytes accessed | tf_op | source)
XLA Modules:
  0.0 426.6 jit_solution(3495875526330565725)
XLA Ops:
  6.5 3.0 collective-permute-start
  11.3 26.4 %all_gather.21 = f32[2048,2]{0,1:T(2,128)S(1)} all-gather(f32[256,2]{0,1:T(2,128)S(1)} %bitcast.168), channel_id=1, replica_groups=mesh['sp'=8,'tp'=4] {'sp'}, dimensions={0}, use_global_device_ids=true | all-gather | bytes 18432 | tf_op jit(solution)/shard_map/all_gather | solution.py:99
  39.1 33.6 %all_gather.20 = bf16[2048,128]{0,1:T(8,128)(2,1)} all-gather(bf16[256,128]{0,1:T(8,128)(2,1)S(1)} %copy.47), channel_id=1, replica_groups=mesh['sp'=8,'tp'=4] {'sp'}, dimensions={0}, use_global_device_ids=true | all-gather | bytes 589824 | tf_op jit(solution)/shard_map/all_gather | solution.py:128
  73.6 31.6 %all_gather.22 = bf16[2048,128]{0,1:T(8,128)(2,1)S(1)} all-gather(bf16[256,128]{0,1:T(8,128)(2,1)S(1)} %copy.49), channel_id=1, replica_groups=mesh['sp'=8,'tp'=4] {'sp'}, dimensions={0}, use_global_device_ids=true | all-gather | bytes 589824 | tf_op jit(solution)/shard_map/all_gather | solution.py:129
  105.2 31.4 %all_gather.19 = bf16[2048,128]{1,0:T(8,128)(2,1)S(1)} all-gather(bf16[256,128]{1,0:T(8,128)(2,1)} %param.24), channel_id=1, replica_groups=mesh['sp'=8,'tp'=4] {'sp'}, dimensions={0}, use_global_device_ids=true | all-gather | bytes 589824 | tf_op jit(solution)/shard_map/all_gather | solution.py:127
  137.3 6.3 %collective-permute-done.1 = bf16[256,128]{1,0:T(8,128)(2,1)S(1)} collective-permute-done((bf16[256,128]{1,0:T(8,128)(2,1)S(1)}, bf16[256,128]{1,0:T(8,128)(2,1)S(1)}, u32[]{:S(2)}, u32[]{:S(2)}) %collective-permute-start.1) | collective-permute-done | bytes 65568 | tf_op jit(solution)/shard_map/ppermute | solution.py:17
  143.9 6.6 %collective-permute-done.2 = bf16[256,128]{1,0:T(8,128)(2,1)S(1)} collective-permute-done((bf16[256,128]{1,0:T(8,128)(2,1)S(1)}, bf16[256,128]{1,0:T(8,128)(2,1)S(1)}, u32[]{:S(2)}, u32[]{:S(2)}) %collective-permute-start.2) | collective-permute-done | bytes 65568 | tf_op jit(solution)/shard_map/ppermute | solution.py:17
  151.4 6.1 %collective-permute-done.3 = bf16[256,128]{1,0:T(8,128)(2,1)S(1)} collective-permute-done((bf16[256,128]{1,0:T(8,128)(2,1)S(1)}, bf16[256,128]{1,0:T(8,128)(2,1)S(1)}, u32[]{:S(2)}, u32[]{:S(2)}) %collective-permute-start.3) | collective-permute-done | bytes 65568 | tf_op jit(solution)/shard_map/ppermute | solution.py:17
  158.9 21.0 %all_gather.18 = f32[2048,1]{0,1:T(1,128)S(1)} all-gather(f32[256,1]{0,1:T(1,128)S(1)} %reduce_window_sum.69), channel_id=1, replica_groups=mesh['sp'=8,'tp'=4] {'sp'}, dimensions={0}, use_global_device_ids=true | all-gather | bytes 9216 | tf_op jit(solution)/shard_map/all_gather | solution.py:98
  184.5 6.4 %collective-permute-done.5 = bf16[256,128]{1,0:T(8,128)(2,1)} collective-permute-done((bf16[256,128]{1,0:T(8,128)(2,1)S(1)}, bf16[256,128]{1,0:T(8,128)(2,1)}, u32[]{:S(2)}, u32[]{:S(2)}) %collective-permute-start.5) | collective-permute-done | bytes 65568 | tf_op jit(solution)/shard_map/ppermute | solution.py:17
  196.0 2.1 collective-permute-done.6
  207.1 9.9 %conditional.2 = (f32[1,128]{1,0:T(1,128)S(1)}, f32[1,128,128]{2,1,0:T(8,128)S(1)}, f32[2,128]{1,0:T(2,128)S(1)}, f32[2,128,64]{1,2,0:T(8,128)}) conditional(s32[]{:T(128)} %convert_element_type.103, (f32[1,128]{1,0:T(1,128)}, f32[1,128,128]{2,1,0:T(8,128)S(1)}, f32[2,128]{1,0:T(2,128)}, f32[2,128,64]{1,2,0:T(8,128)S(1)}) %tuple.35, ...), branch_computations={%region_6.7_spmd, %region_7.12_spmd.clone} | conditional | flops 276104320 | bytes 15037714 | solution.py:180
  217.9 8.7 %conditional.3 = ((f32[1,128]{1,0:T(1,128)}, f32[1,128,128]{2,1,0:T(8,128)S(1)}, f32[2,128]{1,0:T(2,128)}, f32[2,128,64]{1,2,0:T(8,128)S(1)})) conditional(s32[]{:T(128)} %convert_element_type.106, (f32[1,128]{1,0:T(1,128)}, f32[1,128,128]{2,1,0:T(8,128)S(1)}, f32[2,128]{1,0:T(2,128)}, f32[2,128,64]{1,2,0:T(8,128)S(1)}) %tuple.35, ...), branch_computations={%region_12.13_spmd, %region_13.18_spmd.clone} | conditional | flops 276104320 | bytes 15033582 | solution.py:180
  228.5 2.5 fusion.38
  232.1 23.2 %reduce-scatter.3.cloned.1.call-done = bf16[64,2048]{1,0:T(8,128)(2,1)} async-done(((bf16[256,2048]{1,0:T(8,128)(2,1)}), bf16[64,2048]{1,0:T(8,128)(2,1)}) %reduce-scatter.3.cloned.1.call-update) | async-done | bytes 262160 | tf_op jit(solution)/shard_map/reduce_scatter | solution.py:202
  257.9 31.1 %all_to_all.10 = bf16[8,32,2048]{2,1,0:T(8,128)(2,1)} all-to-all(bf16[8,32,2048]{2,1,0:T(8,128)(2,1)S(1)} %bitcast.150), channel_id=1, replica_groups=mesh['sp'=8,'tp'=4] {'sp'}, dimensions={0} | all-to-all | bytes 2097152 | tf_op jit(solution)/shard_map/all_to_all | solution.py:225
  289.3 32.5 %all-gather.2.cloned.1.call-done = bf16[1024,2048]{1,0:T(8,128)(2,1)} async-done(((bf16[256,2048]{1,0:T(8,128)(2,1)}), bf16[1024,2048]{1,0:T(8,128)(2,1)}) %all-gather.2.cloned.1.call-update) | async-done | bytes 4194320 | tf_op jit(solution)/shard_map/all_gather | solution.py:226
  321.8 4.5 %fusion.43 = f32[1024,256]{1,0:T(8,128)} fusion(bf16[1024,2048]{1,0:T(8,128)(2,1)} %all-gather.2.cloned.1.call-done, bf16[1,2048,256]{2,1,0:T(8,128)(2,1)S(1)} %copy-done.24), kind=kOutput, calls=%fused_computation.73 | convolution fusion | flops 1073741824 | bytes 6291456 | tf_op jit(solution)/shard_map/dot_general | solution.py:227
  326.3 9.4 %convolution_convert_fusion = bf16[1024,2048]{1,0:T(8,128)(2,1)} fusion(bf16[1024,2048]{1,0:T(8,128)(2,1)} %all-gather.2.cloned.1.call-done, bf16[1,256,2048]{2,1,0:T(8,128)(2,1)} %param.37, bf16[1,2048,256]{2,1,0:T(8,128)(2,1)} %param.36, f32[1024,256]{1,0:T(8,128)} %fusion.43), kind=kOutput, calls=%fused_computation.65 | convolution fusion | flops 2151153664 | bytes 11534336 | tf_op jit(solution)/shard_map/dot_general | solution.py:231
  335.7 44.7 %reduce-scatter.5.cloned.1.call-done = bf16[256,2048]{1,0:T(8,128)(2,1)} async-done(((bf16[1024,2048]{1,0:T(8,128)(2,1)}), bf16[256,2048]{1,0:T(8,128)(2,1)}) %reduce-scatter.5.cloned.1.call-update) | async-done | bytes 1048592 | tf_op jit(solution)/shard_map/reduce_scatter | solution.py:230
  380.5 5.5 %all-to-all-start.1 = ((bf16[8,32,2048]{2,1,0:T(8,128)(2,1)}), bf16[8,32,2048]{2,1,0:T(8,128)(2,1)S(1)}, u32[]{:S(2)}, u32[]{:S(2)}) async-start(bf16[8,32,2048]{2,1,0:T(8,128)(2,1)} %bitcast.151), calls=%async_computation.3 | async-start | bytes 2097152 | tf_op jit(solution)/shard_map/all_to_all | solution.py:236
  386.4 25.2 %all-to-all-done.1 = bf16[8,32,2048]{2,1,0:T(8,128)(2,1)S(1)} async-done(((bf16[8,32,2048]{2,1,0:T(8,128)(2,1)}), bf16[8,32,2048]{2,1,0:T(8,128)(2,1)S(1)}, u32[]{:S(2)}, u32[]{:S(2)}) %all-to-all-start.1) | async-done | bytes 1048608 | tf_op jit(solution)/shard_map/all_to_all | solution.py:236
  413.4 2.2 gather.7
  415.6 3.6 multiply_reduce_fusion
  (180 shorter events, 53.9 us)
Async XLA Ops:
  6.5 221.5 %copy-start = (bf16[512,2048]{1,0:T(8,128)(2,1)S(1)}, bf16[512,2048]{1,0:T(8,128)(2,1)}, u32[]{:S(2)}) copy-start(bf16[512,2048]{1,0:T(8,128)(2,1)} %param.30) | copy-start | bytes 6291460
  6.5 195.1 %copy-start.5 = (bf16[256,128]{1,0:T(8,128)(2,1)S(1)}, bf16[256,128]{1,0:T(8,128)(2,1)}, u32[]{:S(2)}) copy-start(bf16[256,128]{1,0:T(8,128)(2,1)} %param.23) | copy-start | bytes 196612
  6.5 137.1 %copy-start.20 = (f32[256,1]{0,1:T(1,128)S(1)}, f32[256,1]{0,1:T(1,128)}, u32[]{:S(2)}) copy-start(f32[256,1]{0,1:T(1,128)} %param.28) | copy-start | bytes 3076
  6.5 248.8 %reduce-scatter.3.cloned.1.call-start = ((), (), s32[]{:S(2)}) async-start(), calls=%async_computation.4 | async-start | bytes 1310720 | tf_op jit(solution)/shard_map/reduce_scatter | solution.py:202
  6.5 130.0 %collective-permute-start = (bf16[256,128]{1,0:T(8,128)(2,1)}, bf16[256,128]{1,0:T(8,128)(2,1)S(1)}, u32[]{:S(2)}, u32[]{:S(2)}) collective-permute-start(bf16[256,128]{1,0:T(8,128)(2,1)} %param.23), channel_id=1, source_target_pairs={{0,4},{4,8},{8,12},{12,16},{16,20},{20,24},{24,28},{28,0},{1,5},{5... | collective-permute-start | bytes 196616 | tf_op jit(solution)/shard_map/ppermute | solution.py:17
  136.6 7.0 %collective-permute-start.1 = (bf16[256,128]{1,0:T(8,128)(2,1)S(1)}, bf16[256,128]{1,0:T(8,128)(2,1)S(1)}, u32[]{:S(2)}, u32[]{:S(2)}) collective-permute-start(bf16[256,128]{1,0:T(8,128)(2,1)S(1)} %collective-permute-done), channel_id=1, source_target_pairs={{0,4},{4,8},{8,12},{12,16},{16,20},{20,24},{24,28},{28,0},{1,5},{5... | collective-permute-start | bytes 196616 | tf_op jit(solution)/shard_map/ppermute | solution.py:17
  143.6 7.0 %collective-permute-start.2 = (bf16[256,128]{1,0:T(8,128)(2,1)S(1)}, bf16[256,128]{1,0:T(8,128)(2,1)S(1)}, u32[]{:S(2)}, u32[]{:S(2)}) collective-permute-start(bf16[256,128]{1,0:T(8,128)(2,1)S(1)} %collective-permute-done.1), channel_id=1, source_target_pairs={{0,4},{4,8},{8,12},{12,16},{16,20},{20,24},{24,28},{28,0},{1,5},{5... | collective-permute-start | bytes 196616 | tf_op jit(solution)/shard_map/ppermute | solution.py:17
  143.9 7.5 %copy-start.18 = (f32[1,2,128]{2,1,0:T(2,128)}, f32[1,2,128]{2,1,0:T(2,128)S(1)}, u32[]{:S(2)}) copy-start(f32[1,2,128]{2,1,0:T(2,128)S(1)} %reduce-window.14) | copy-start | bytes 3076
  150.6 7.0 %collective-permute-start.3 = (bf16[256,128]{1,0:T(8,128)(2,1)S(1)}, bf16[256,128]{1,0:T(8,128)(2,1)S(1)}, u32[]{:S(2)}, u32[]{:S(2)}) collective-permute-start(bf16[256,128]{1,0:T(8,128)(2,1)S(1)} %collective-permute-done.2), channel_id=1, source_target_pairs={{0,4},{4,8},{8,12},{12,16},{16,20},{20,24},{24,28},{28,0},{1,5},{5... | collective-permute-start | bytes 196616 | tf_op jit(solution)/shard_map/ppermute | solution.py:17
  157.5 37.3 %copy-start.6 = (bf16[256,128]{1,0:T(8,128)(2,1)}, bf16[256,128]{1,0:T(8,128)(2,1)S(1)}, u32[]{:S(2)}) copy-start(bf16[256,128]{1,0:T(8,128)(2,1)S(1)} %collective-permute-done.3) | copy-start | bytes 196612
  157.5 26.2 %collective-permute-start.4 = (bf16[256,128]{1,0:T(8,128)(2,1)S(1)}, bf16[256,128]{1,0:T(8,128)(2,1)S(1)}, u32[]{:S(2)}, u32[]{:S(2)}) collective-permute-start(bf16[256,128]{1,0:T(8,128)(2,1)S(1)} %collective-permute-done.3), channel_id=1, source_target_pairs={{0,4},{4,8},{8,12},{12,16},{16,20},{20,24},{24,28},{28,0},{1,5},{5... | collective-permute-start | bytes 196616 | tf_op jit(solution)/shard_map/ppermute | solution.py:17
  183.8 11.1 %copy-start.7 = (bf16[256,128]{1,0:T(8,128)(2,1)}, bf16[256,128]{1,0:T(8,128)(2,1)S(1)}, u32[]{:S(2)}) copy-start(bf16[256,128]{1,0:T(8,128)(2,1)S(1)} %collective-permute-done.4) | copy-start | bytes 196612
  183.8 7.1 %collective-permute-start.5 = (bf16[256,128]{1,0:T(8,128)(2,1)S(1)}, bf16[256,128]{1,0:T(8,128)(2,1)}, u32[]{:S(2)}, u32[]{:S(2)}) collective-permute-start(bf16[256,128]{1,0:T(8,128)(2,1)S(1)} %collective-permute-done.4), channel_id=1, source_target_pairs={{0,4},{4,8},{8,12},{12,16},{16,20},{20,24},{24,28},{28,0},{1,5},{5... | collective-permute-start | bytes 196616 | tf_op jit(solution)/shard_map/ppermute | solution.py:17
  190.9 7.3 %collective-permute-start.6 = (bf16[256,128]{1,0:T(8,128)(2,1)}, bf16[256,128]{1,0:T(8,128)(2,1)}, u32[]{:S(2)}, u32[]{:S(2)}) collective-permute-start(bf16[256,128]{1,0:T(8,128)(2,1)} %collective-permute-done.5), channel_id=1, source_target_pairs={{0,4},{4,8},{8,12},{12,16},{16,20},{20,24},{24,28},{28,0},{1,5},{5... | collective-permute-start | bytes 196616 | tf_op jit(solution)/shard_map/ppermute | solution.py:17
  192.8 14.3 %copy-start.9 = (f32[2048,2]{0,1:T(2,128)S(1)}, f32[2048,2]{0,1:T(2,128)}, u32[]{:S(2)}) copy-start(f32[2048,2]{0,1:T(2,128)} %add.317) | copy-start | bytes 49156
  218.0 3.8 copy-start.11
  228.5 26.9 %copy-start.1 = (bf16[64,2048]{1,0:T(8,128)(2,1)S(1)}, bf16[64,2048]{1,0:T(8,128)(2,1)}, u32[]{:S(2)}) copy-start(bf16[64,2048]{1,0:T(8,128)(2,1)} %param.21) | copy-start | bytes 786436
  228.5 28.0 %copy-start.13 = (f32[2048]{0:T(1024)S(1)}, f32[2048]{0:T(1024)}, u32[]{:S(2)}) copy-start(f32[2048]{0:T(1024)} %param.32) | copy-start | bytes 24580
  231.1 90.7 %all-gather.2.cloned.1.call-start = ((), (), s32[]{:S(2)}) async-start(), calls=%async_computation.5 | async-start | bytes 5242880 | tf_op jit(solution)/shard_map/all_gather | solution.py:226
  257.9 63.9 %copy-start.24 = (bf16[1,2048,256]{2,1,0:T(8,128)(2,1)S(1)}, bf16[1,2048,256]{2,1,0:T(8,128)(2,1)}, u32[]{:S(2)}) copy-start(bf16[1,2048,256]{2,1,0:T(8,128)(2,1)} %param.35) | copy-start | bytes 3145732
  289.1 91.4 %reduce-scatter.5.cloned.1.call-start = ((), (), s32[]{:S(2)}) async-start(), calls=%async_computation.6 | async-start | bytes 5242880 | tf_op jit(solution)/shard_map/reduce_scatter | solution.py:230
  335.7 50.6 %copy-start.19 = (f32[64,2]{0,1:T(2,128)S(1)}, f32[64,2]{0,1:T(2,128)}, u32[]{:S(2)}) copy-start(f32[64,2]{0,1:T(2,128)} %param.34) | copy-start | bytes 1540
  380.5 31.2 %all-to-all-start.1 = ((bf16[8,32,2048]{2,1,0:T(8,128)(2,1)}), bf16[8,32,2048]{2,1,0:T(8,128)(2,1)S(1)}, u32[]{:S(2)}, u32[]{:S(2)}) async-start(bf16[8,32,2048]{2,1,0:T(8,128)(2,1)} %bitcast.151), calls=%async_computation.3 | async-start | bytes 2097152 | tf_op jit(solution)/shard_map/all_to_all | solution.py:236
  413.3 5.9 %copy-start.2 = (bf16[64,2048]{1,0:T(8,128)(2,1)S(1)}, bf16[64,2048]{1,0:T(8,128)(2,1)}, u32[]{:S(2)}) copy-start(bf16[64,2048]{1,0:T(8,128)(2,1)} %reduce-scatter.3.cloned.1.call-done) | copy-start | bytes 786436
  (14 other events, 27.0 us)
Sparse Core Ops, SparseCore 0:
  231.2 24.1 reduce-scatter.2
  289.2 32.5 all-gather.1
  335.8 44.5 reduce-scatter.4
